TPU v7x, 128 devices: a whole 4x4x4 slice. The times are simulated.
128 devices in a mesh: sp: 32 (over z, y, core), tp: 4 (over x).
Axes of the slice: x: 4, y: 4, z: 4, core: 2. Of those that a mesh axis runs over, the one named last changes fastest.
Arguments:
- tokens: bfloat16 [32768, 2048], P('sp', 'tp'), may hold values from -6 to 6
- input_norm_gain: float32 [2048], replicated, may hold values from 0.1 to 1.9
- pooling_input_matrix: bfloat16 [2048, 512], P(None, 'tp'), may hold values from -0.125 to 0.125
- query_projection_matrix: bfloat16 [2048, 1024], P(None, 'tp'), may hold values from -0.125 to 0.125
- key_projection_matrix: bfloat16 [2048, 1024], P(None, 'tp'), may hold values from -0.125 to 0.125
- value_projection_matrix: bfloat16 [2048, 1024], P(None, 'tp'), may hold values from -0.125 to 0.125
- output_gate_matrix: bfloat16 [2048, 1024], P(None, 'tp'), may hold values from -0.125 to 0.125
- input_gate_matrix: bfloat16 [2048, 2, 8], replicated
- forget_gate_matrix: bfloat16 [2048, 2, 8], replicated, may hold values from -0.125 to 0.125
- forget_gate_bias: float32 [2, 8], replicated
- log_forget_scale: float32 [2, 32768], P(None, 'sp'), may hold values from 0.35 to 2.8
- extra_log_forget: float32 [2, 32768], P(None, 'sp'), may hold values from -0.7 to 0, as said below
- starting_memory: float32 [2, 8, 128, 128], P(None, 'tp'), may hold values from -3 to 3
- starting_normalizer: float32 [2, 8, 128], P(None, 'tp'), may hold values from -3 to 3
- starting_log_scale: float32 [2, 8], P(None, 'tp'), may hold values from 2 to 5
- pooling_group_map: bfloat16 [4, 128, 128], replicated, may hold values from -0.5 to 0.5
- pooling_channel_scale: float32 [512], replicated, may hold values from 0.1 to 1.9
- memory_head_gain: float32 [1024], replicated, may hold values from 0.1 to 1.9
- pooling_output_matrix: bfloat16 [512, 2048], replicated, may hold values from -0.25 to 0.25
- memory_output_matrix: bfloat16 [1024, 2048], replicated, may hold values from -0.1875 to 0.1875
Outputs:
- mixed_out: bfloat16 [32768, 2048], P(('sp', 'tp'))
Inputs may be any that keep to these rules, and one draw needn't show every extreme that they name: `extra_log_forget`: at most three nonzero entries in each direction.
All inputs are finite; a program needn't handle non-finite values.
Results may differ from a plain program's by a relative error of at most 0.0091.
Values may be sent and summed in bfloat16 or wider, within the bound.
A program may use at most 128 MiB of HBM per device.

v0:
```python
import jax
import jax.numpy as jnp
from jax import lax
from jax.sharding import PartitionSpec as P

DH = 128
BLOCK = 128
NEG_BIG = -1e30
LN_EPS = 1e-05
HEAD_EPS = 1e-06
RIM_ROWS = 8


def extended(block, sides, width):
    for axis, dim in sides:
        count = lax.axis_size(axis)
        forward = [(i, i + 1) for i in range(count - 1)]
        backward = [(target, source) for source, target in forward]
        low = lax.ppermute(
            lax.slice_in_dim(block, block.shape[dim] - width, None, axis=dim), axis, forward
        )
        high = lax.ppermute(lax.slice_in_dim(block, 0, width, axis=dim), axis, backward)
        block = jnp.concatenate([low, block, high], axis=dim)
    return block


def block_step(carried, pieces):
    memory, normer, maxlog = carried
    q_blk, k_blk, v_blk, i_blk, f_blk = pieces
    lower_mask = jnp.tril(jnp.ones((BLOCK, BLOCK), dtype=bool))
    cumulative = jnp.cumsum(f_blk, axis=-1)
    exponent = jnp.where(
        lower_mask, cumulative[:, :, None] - cumulative[:, None, :] + i_blk[:, None, :], NEG_BIG
    )
    carried_log = cumulative + maxlog[:, None]
    row_max = jnp.maximum(carried_log, exponent.max(-1))
    fading = jnp.exp(carried_log - row_max)
    scores = jnp.einsum("htd,hsd->hts", q_blk, k_blk) * jnp.exp(exponent - row_max[:, :, None])
    numerator = fading[:, :, None] * jnp.einsum("hvk,htk->htv", memory, q_blk) + jnp.einsum(
        "hts,hsv->htv", scores, v_blk
    )
    denominator = fading * jnp.einsum("hk,htk->ht", normer, q_blk) + scores.sum(-1)
    summed = cumulative[:, -1]
    weight_log = summed[:, None] - cumulative + i_blk
    new_max = jnp.maximum(summed + maxlog, weight_log.max(-1))
    carry_scale = jnp.exp(summed + maxlog - new_max)
    weights = jnp.exp(weight_log - new_max[:, None])
    memory = carry_scale[:, None, None] * memory + jnp.einsum(
        "hsv,hsk->hvk", v_blk * weights[:, :, None], k_blk
    )
    normer = carry_scale[:, None] * normer + jnp.einsum("hs,hsk->hk", weights, k_blk)
    return ((memory, normer, new_max), (numerator, denominator, row_max))


def to_blocks(source):
    return jnp.moveaxis(
        source.reshape((source.shape[0], source.shape[1] // BLOCK, BLOCK) + source.shape[2:]), 1, 0
    )


def from_blocks(source):
    return jnp.moveaxis(source, 0, 1).reshape(
        (source.shape[1], source.shape[0] * source.shape[2]) + source.shape[3:]
    )


def local_pass(query_heads, key_heads, value_heads, log_in, log_forget_gate):
    head_count = query_heads.shape[0]
    head_size = query_heads.shape[2]
    initial = (
        jnp.zeros((head_count, head_size, head_size), jnp.float32),
        jnp.zeros((head_count, head_size), jnp.float32),
        jnp.full((head_count,), NEG_BIG, jnp.float32),
    )
    finals, outputs = lax.scan(
        block_step,
        initial,
        tuple(
            (
                to_blocks(member)
                for member in (query_heads, key_heads, value_heads, log_in, log_forget_gate)
            )
        ),
    )
    numerator, denominator, row_max = (from_blocks(member) for member in outputs)
    falls = jnp.cumsum(log_forget_gate, axis=1)
    return ((falls[:, -1],) + finals, (numerator, denominator, row_max, falls))


def join_states(earlier, later):
    early_fall, early_memory, early_normer, early_max = earlier
    late_fall, late_memory, late_normer, late_max = later
    merged_max = jnp.maximum(early_max + late_fall, late_max)
    early_weight = jnp.exp(early_max + late_fall - merged_max)
    late_weight = jnp.exp(late_max - merged_max)
    return (
        late_fall,
        early_weight[..., None, None] * early_memory + late_weight[..., None, None] * late_memory,
        early_weight[..., None] * early_normer + late_weight[..., None] * late_normer,
        merged_max,
    )


def prefix_from_all(gathered, position, from_later):
    falls, memories, normers, maxima = gathered
    order = jnp.arange(falls.shape[0], dtype=jnp.int32)
    inclusive = jnp.cumsum(falls, axis=0)
    exclusive = inclusive - falls
    if from_later:
        valid = order > position
        between = exclusive - inclusive[position][None]
        total_fall = inclusive[-1] - inclusive[position]
    else:
        valid = order < position
        between = exclusive[position][None] - inclusive
        total_fall = exclusive[position]
    log_weight = jnp.where(valid[:, None], maxima + between, NEG_BIG)
    joint_max = jnp.max(log_weight, axis=0)
    weights = jnp.where(valid[:, None], jnp.exp(log_weight - joint_max[None]), 0.0)
    memory = jnp.einsum("jh,jhvk->hvk", weights, memories)
    normer = jnp.einsum("jh,jhk->hk", weights, normers)
    return (total_fall, memory, normer, joint_max)


def finish(local_terms, entering, query_heads):
    numerator, denominator, row_max, falls = local_terms
    fall_in, memory, normer, max_in = entering
    state_log = falls + max_in[:, None]
    joint_max = jnp.maximum(row_max, state_log)
    local_weight = jnp.exp(row_max - joint_max)
    state_weight = jnp.exp(state_log - joint_max)
    full_numerator = local_weight[..., None] * numerator + state_weight[..., None] * jnp.einsum(
        "hvk,htk->htv", memory, query_heads
    )
    full_denominator = local_weight * denominator + state_weight * jnp.einsum(
        "hk,htk->ht", normer, query_heads
    )
    return full_numerator / jnp.maximum(jnp.abs(full_denominator), 1.0)[..., None]


def per_device(
    tokens,
    input_norm_gain,
    pooling_input_matrix,
    query_projection_matrix,
    key_projection_matrix,
    value_projection_matrix,
    output_gate_matrix,
    input_gate_matrix,
    forget_gate_matrix,
    forget_gate_bias,
    log_forget_scale,
    extra_log_forget,
    starting_memory,
    starting_normalizer,
    starting_log_scale,
    pooling_group_map,
    pooling_channel_scale,
    memory_head_gain,
    pooling_output_matrix,
    memory_output_matrix,
):
    local_rows = tokens.shape[0]
    own_width = tokens.shape[1]
    model_width = own_width * lax.axis_size("tp")
    group_index = lax.axis_index("tp")
    seq_index = lax.axis_index("sp")
    group_dim = pooling_input_matrix.shape[1]
    head_local = query_projection_matrix.shape[1] // DH
    mem_width = head_local * DH
    main_weight = jnp.concatenate(
        [
            pooling_input_matrix,
            query_projection_matrix,
            key_projection_matrix,
            value_projection_matrix,
            output_gate_matrix,
        ],
        axis=1,
    )
    gate_in = lax.dynamic_slice_in_dim(input_gate_matrix, group_index * head_local, head_local, 2)
    gate_fg = lax.dynamic_slice_in_dim(forget_gate_matrix, group_index * head_local, head_local, 2)
    gate_weight = jnp.concatenate([gate_in, gate_fg], axis=1).reshape(model_width, 4 * head_local)
    whole_rows = lax.all_gather(tokens, "tp", axis=1, tiled=True)
    floats = whole_rows.astype(jnp.float32)
    mean_row = jnp.sum(floats, axis=1) / model_width
    variance = jnp.sum(floats * floats, axis=1) / model_width - mean_row * mean_row
    normed = (
        (floats - mean_row[:, None]) * lax.rsqrt(variance + LN_EPS)[:, None] * input_norm_gain
    ).astype(jnp.bfloat16)
    projected = jnp.dot(normed, main_weight, preferred_element_type=jnp.float32)
    gate_pre = jnp.dot(normed, gate_weight, preferred_element_type=jnp.float32)
    pool_in = projected[:, :group_dim].astype(jnp.bfloat16)
    queries = projected[:, group_dim : group_dim + mem_width].astype(jnp.bfloat16)
    key_rows = projected[:, group_dim + mem_width : group_dim + 2 * mem_width].astype(jnp.bfloat16)
    value_rows = projected[:, group_dim + 2 * mem_width : group_dim + 3 * mem_width].astype(
        jnp.bfloat16
    )
    out_gate = projected[:, group_dim + 3 * mem_width :].astype(jnp.bfloat16)
    gate_pre = gate_pre.reshape(local_rows, 2, 2, head_local)
    log_in = gate_pre[:, 0]
    bias_own = lax.dynamic_slice_in_dim(forget_gate_bias, group_index * head_local, head_local, 1)
    log_forget_gate = (
        jax.nn.log_sigmoid(gate_pre[:, 1] + bias_own[None]) * log_forget_scale.T[:, :, None]
        + extra_log_forget.T[:, :, None]
    )

    def heads_of(source, factor):
        return (
            (source.astype(jnp.float32) * factor)
            .reshape(local_rows, head_local, DH)
            .transpose(1, 0, 2)
        )

    query_heads = heads_of(queries, 1.0)
    key_heads = heads_of(key_rows, DH ** (-0.5))
    value_heads = heads_of(value_rows, 1.0)
    forward_summary, forward_local = local_pass(
        query_heads, key_heads, value_heads, log_in[:, 0].T, log_forget_gate[:, 0].T
    )
    flipped_query = query_heads[:, ::-1]
    backward_summary, backward_local = local_pass(
        flipped_query,
        key_heads[:, ::-1],
        value_heads[:, ::-1],
        log_in[:, 1].T[:, ::-1],
        log_forget_gate[:, 1].T[:, ::-1],
    )
    rimmed = extended(pool_in, (("sp", 0),), RIM_ROWS).astype(jnp.float32)
    half_span = jnp.left_shift(jnp.int32(1), group_index)
    grouped = pool_in.astype(jnp.float32)
    pooled = jnp.zeros_like(grouped)
    for offset in range(-RIM_ROWS, RIM_ROWS):
        inside = ((offset >= -half_span) & (offset < half_span)).astype(jnp.float32)
        pooled = pooled + inside * rimmed[RIM_ROWS + offset : RIM_ROWS + offset + local_rows]
    positions = seq_index * local_rows + jnp.arange(local_rows, dtype=jnp.int32)
    total_rows = local_rows * lax.axis_size("sp")
    counts = (
        jnp.minimum(positions + half_span, total_rows) - jnp.maximum(positions - half_span, 0)
    ).astype(jnp.float32)
    contrast = (pooled / counts[:, None] - grouped).astype(jnp.bfloat16)
    map_own = lax.dynamic_index_in_dim(pooling_group_map, group_index, 0, keepdims=False)
    scale_own = lax.dynamic_slice_in_dim(
        pooling_channel_scale, group_index * group_dim, group_dim, 0
    )
    pool_out = (jnp.dot(contrast, map_own, preferred_element_type=jnp.float32) * scale_own).astype(
        jnp.bfloat16
    )
    stacked = tuple(
        (
            jnp.stack([forward_part, backward_part])[None]
            for forward_part, backward_part in zip(forward_summary, backward_summary)
        )
    )
    gathered = lax.all_gather(stacked, "sp", axis=0, tiled=True)
    forward_prefix = prefix_from_all(tuple((member[:, 0] for member in gathered)), seq_index, False)
    backward_prefix = prefix_from_all(tuple((member[:, 1] for member in gathered)), seq_index, True)

    def initial_state(direction):
        return (
            jnp.zeros((head_local,), jnp.float32),
            starting_memory[direction],
            starting_normalizer[direction],
            starting_log_scale[direction],
        )

    forward = finish(forward_local, join_states(initial_state(0), forward_prefix), query_heads)
    backward = finish(backward_local, join_states(initial_state(1), backward_prefix), flipped_query)
    hidden = forward + backward[:, ::-1]
    head_mean = jnp.mean(hidden, axis=-1, keepdims=True)
    head_var = jnp.mean(jnp.square(hidden - head_mean), axis=-1, keepdims=True)
    gain_heads = lax.dynamic_slice_in_dim(
        memory_head_gain, group_index * mem_width, mem_width, 0
    ).reshape(head_local, DH)
    scaled = (hidden - head_mean) * lax.rsqrt(head_var + HEAD_EPS) * gain_heads[:, None, :]
    mem_out = (
        scaled.transpose(1, 0, 2).reshape(local_rows, mem_width)
        * jax.nn.sigmoid(out_gate.astype(jnp.float32))
    ).astype(jnp.bfloat16)
    mixed = jnp.concatenate([pool_out, mem_out], axis=1)
    owned = lax.all_to_all(mixed, "tp", split_axis=0, concat_axis=1, tiled=True)
    owner_rows = owned.shape[0]
    owned = owned.reshape(owner_rows, lax.axis_size("tp"), group_dim + mem_width)
    pool_part = owned[:, :, :group_dim].reshape(owner_rows, lax.axis_size("tp") * group_dim)
    mem_part = owned[:, :, group_dim:].reshape(owner_rows, lax.axis_size("tp") * mem_width)
    result = jnp.dot(
        pool_part, pooling_output_matrix, preferred_element_type=jnp.float32
    ) + jnp.dot(mem_part, memory_output_matrix, preferred_element_type=jnp.float32)
    return result.astype(jnp.bfloat16)


def solution(mesh):
    placed = (
        P("sp", "tp"),
        P(),
        P(None, "tp"),
        P(None, "tp"),
        P(None, "tp"),
        P(None, "tp"),
        P(None, "tp"),
        P(),
        P(),
        P(),
        P(None, "sp"),
        P(None, "sp"),
        P(None, "tp", None, None),
        P(None, "tp", None),
        P(None, "tp"),
        P(),
        P(),
        P(),
        P(),
        P(),
    )
    return jax.shard_map(
        per_device, mesh=mesh, in_specs=placed, out_specs=P(("sp", "tp"), None), check_vma=False
    )
```

profile of v0, /device:TPU:1, one launch (start us, length us, event | category | flops | bytes accessed | tf_op | source)
XLA Modules:
  0.0 383.7 jit_solution(3305362146877481871)
XLA Ops:
  9.4 1.9 constant_dynamic-update-slice_fusion.8
  11.3 2.3 constant_dynamic-update-slice_fusion.7
  16.9 43.3 %all-gather.9.cloned.1.call-done = bf16[1024,2048]{1,0:T(8,128)(2,1)} async-done(((bf16[1024,512]{1,0:T(8,128)(2,1)}), bf16[1024,2048]{1,0:T(8,128)(2,1)}) %all-gather.9.cloned.1.call-update) | async-done | bytes 4194320 | tf_op jit(solution)/shard_map/all_gather | solution.py:184
  60.2 3.6 convert_reduce_fusion
  63.9 8.5 %convolution_convert_fusion = bf16[1024,1152]{1,0:T(8,128)(2,1)S(1)} fusion(bf16[2048,1152]{1,0:T(8,128)(2,1)} %constant_dynamic-update-slice_fusion.4, bf16[1024,2048]{1,0:T(8,128)(2,1)S(1)} %copy-done.5, f32[2048]{0:T(1024)S(1)} %copy-done.21, f32[1024]{0:T(1024)S(1)} %get-tuple-element.398, f32[1024]{0:T(1024)S(1)} %get-tuple-element.397), kind=kOutput, calls=%fused_computation.125 | convolution fusion | flops 4843503616 | bytes 11288576 | tf_op jit(solution)/shard_map/dot_general | solution.py:191
  75.9 5.1 %rev.22 = bf16[2,1024,128]{2,1,0:T(8,128)(2,1)} reverse(bf16[2,1024,128]{2,1,0:T(8,128)(2,1)S(1)} %get-tuple-element.407), dimensions={1} | reverse | bytes 1048576 | tf_op jit(solution)/shard_map/rev | solution.py:221
  81.0 3.7 fusion.70
  87.6 5.1 %rev.20 = f32[2,1024,128]{2,1,0:T(8,128)} reverse(f32[2,1024,128]{2,1,0:T(8,128)S(1)} %bitcast.498), dimensions={1} | reverse | bytes 2097152 | tf_op jit(solution)/shard_map/rev | solution.py:225
  92.7 8.2 %rev.21 = bf16[2,1024,128]{2,1,0:T(8,128)(2,1)} reverse(bf16[2,1024,128]{2,1,0:T(8,128)(2,1)} %get-tuple-element.381), dimensions={1} | reverse | bytes 1048576 | tf_op jit(solution)/shard_map/rev | solution.py:224
  101.0 1.9 copy.212
  104.0 66.0 %while.43 = (s32[]{:T(128)}, f32[2,128,128]{2,1,0:T(8,128)S(1)}, f32[2,128]{1,0:T(2,128)S(1)}, f32[2]{0:T(128)S(1)}, f32[8,2,128,128]{3,2,1,0:T(8,128)}, /*index...) while((s32[]{:T(128)}, f32[2,128,128]{2,1,0:T(8,128)S(1)}, ...), condition=%wide.region_18.19_spmd.clone, body=%wide.region_13.18_spmd.clone.sunk | while | flops 34327816 | bytes 1600317 | solution.py:75
  126.9 1.8 fusion.266
  135.1 1.8 fusion.266
  143.4 1.8 fusion.266
  159.9 1.8 fusion.266
  169.9 1.9 copy.213
  172.9 58.1 %while.42 = (s32[]{:T(128)}, f32[2,128,128]{2,1,0:T(8,128)S(1)}, f32[2,128]{1,0:T(2,128)S(1)}, f32[2]{0:T(128)S(1)}, f32[8,2,128,128]{3,2,1,0:T(8,128)}, /*index...) while((s32[]{:T(128)}, f32[2,128,128]{2,1,0:T(8,128)S(1)}, ...), condition=%wide.region_7.8_spmd.clone, body=%wide.region_2.7_spmd.clone.sunk | while | flops 34327816 | bytes 1600821 | solution.py:75
  236.3 25.2 %all-gather.4 = f32[32,2,2]{2,1,0:T(2,128)S(1)} all-gather(f32[1,2,2]{2,1,0:T(2,128)S(1)} %maximum_bitcast_fusion), channel_id=2, replica_groups=mesh['sp'=32,'tp'=4] {'sp'}, dimensions={0}, use_global_device_ids=true | all-gather | bytes 528 | tf_op jit(solution)/shard_map/all_gather | solution.py:255
  261.7 23.6 %all-gather.5 = f32[32,2,2]{2,1,0:T(2,128)S(1)} all-gather(f32[1,2,2]{2,1,0:T(2,128)S(1)} %maximum_bitcast_fusion.1), channel_id=3, replica_groups=mesh['sp'=32,'tp'=4] {'sp'}, dimensions={0}, use_global_device_ids=true | all-gather | bytes 528 | tf_op jit(solution)/shard_map/all_gather | solution.py:255
  286.8 2.1 collective-permute-start.1
  288.9 3.5 collective-permute-start
  292.4 22.6 %all-gather.3 = bf16[64,2,128]{2,1,0:T(2,128)(2,1)S(1)} all-gather(bf16[2,2,128]{2,1,0:T(2,128)(2,1)S(1)} %pad_maximum_fusion.3), channel_id=5, replica_groups=mesh['sp'=32,'tp'=4] {'sp'}, dimensions={0}, use_global_device_ids=true | all-gather | bytes 33792 | tf_op jit(solution)/shard_map/all_gather | solution.py:255
  318.4 2.6 copy.115
  321.0 2.4 reshape.649
  324.9 2.4 reshape.646
  327.4 2.1 fusion.82
  329.5 4.2 %slice_bitcast_fusion.1 = (bf16[32,2,128,128]{3,2,1,0:T(8,128)(2,1)}, bf16[32,2,128,128]{3,2,1,0:T(8,128)(2,1)S(1)}) fusion(bf16[32,2,2,128,128]{4,3,2,1,0:T(8,128)(2,1)} %bitcast.502), kind=kLoop, calls=%fused_computation.118 | loop fusion | bytes 8388608 | tf_op jit(solution)/shard_map/squeeze | solution.py:256
  336.4 9.4 %rev.23 = f32[2,1024,128]{1,2,0:T(8,128)} reverse(f32[2,1024,128]{1,2,0:T(8,128)} %fusion.81), dimensions={1} | reverse | bytes 2097152 | tf_op jit(solution)/shard_map/rev | solution.py:269
  345.7 2.8 fusion.74
  348.6 2.0 fusion.176
  356.0 15.5 %all_to_all.16 = bf16[4,256,384]{1,2,0:T(8,128)(2,1)S(1)} all-to-all(bf16[4,256,384]{1,2,0:T(8,128)(2,1)} %copy.118), channel_id=1, replica_groups=mesh['sp'=32,'tp'=4] {'tp'}, dimensions={0} | all-to-all | bytes 1572864 | tf_op jit(solution)/shard_map/all_to_all | solution.py:281
  371.6 3.5 fusion.178
  (438 shorter events, 152.4 us)
Async XLA Ops:
  6.5 368.6 %copy-start = (bf16[512,2048]{1,0:T(8,128)(2,1)S(1)}, bf16[512,2048]{1,0:T(8,128)(2,1)}, u32[]{:S(2)}) copy-start(bf16[512,2048]{1,0:T(8,128)(2,1)} %param.42) | copy-start | bytes 6291460
  6.5 7.1 %copy-start.8 = (bf16[2048,256]{1,0:T(8,128)(2,1)S(1)}, bf16[2048,256]{1,0:T(8,128)(2,1)}, u32[]{:S(2)}) copy-start(bf16[2048,256]{1,0:T(8,128)(2,1)} %param.28) | copy-start | bytes 3145732
  6.5 53.7 %all-gather.9.cloned.1.call-start = ((), (), s32[]{:S(2)}) async-start(), calls=%async_computation.1 | async-start | bytes 5242880 | tf_op jit(solution)/shard_map/all_gather | solution.py:184
  7.3 322.2 %all-gather.11.cloned.1.call-start = ((), (), s32[]{:S(2)}) async-start(), calls=%async_computation.2 | async-start | bytes 4325376 | tf_op jit(solution)/shard_map/all_gather | solution.py:255
  8.4 6.2 %copy-start.9 = (bf16[2048,256]{1,0:T(8,128)(2,1)S(1)}, bf16[2048,256]{1,0:T(8,128)(2,1)}, u32[]{:S(2)}) copy-start(bf16[2048,256]{1,0:T(8,128)(2,1)} %param.29) | copy-start | bytes 3145732
  8.5 7.3 %copy-start.10 = (bf16[2048,256]{1,0:T(8,128)(2,1)S(1)}, bf16[2048,256]{1,0:T(8,128)(2,1)}, u32[]{:S(2)}) copy-start(bf16[2048,256]{1,0:T(8,128)(2,1)} %param.30) | copy-start | bytes 3145732
  14.7 49.2 %copy-start.21 = (f32[2048]{0:T(1024)S(1)}, f32[2048]{0:T(1024)}, u32[]{:S(2)}) copy-start(f32[2048]{0:T(1024)} %param.25) | copy-start | bytes 24580
  60.2 3.6 copy-start.5
  72.4 3.5 copy-start.7
  73.9 0.8 copy-start.1
  75.9 8.8 %copy-start.3 = (bf16[2,1024,128]{2,1,0:T(8,128)(2,1)}, bf16[2,1024,128]{2,1,0:T(8,128)(2,1)S(1)}, u32[]{:S(2)}) copy-start(bf16[2,1024,128]{2,1,0:T(8,128)(2,1)S(1)} %get-tuple-element.407) | copy-start | bytes 1572868
  81.0 3.7 copy-start.12
  81.0 3.7 copy-start.13
  172.9 113.0 %copy-start.15 = (f32[2,2]{1,0:T(2,128)S(1)}, f32[2,2]{1,0:T(2,128)}, u32[]{:S(2)}) copy-start(f32[2,2]{1,0:T(2,128)} %param.38) | copy-start | bytes 52
  172.9 142.5 %copy-start.14 = (f32[2,2,128]{2,1,0:T(2,128)S(1)}, f32[2,2,128]{2,1,0:T(2,128)}, u32[]{:S(2)}) copy-start(f32[2,2,128]{2,1,0:T(2,128)} %param.37) | copy-start | bytes 6148
  231.0 92.6 %copy-start.6 = (f32[8,2,128,128]{3,2,1,0:T(8,128)S(1)}, f32[8,2,128,128]{3,2,1,0:T(8,128)}, u32[]{:S(2)}) copy-start(f32[8,2,128,128]{3,2,1,0:T(8,128)} %get-tuple-element.142) | copy-start | bytes 3145732
  286.8 40.5 %collective-permute-start.1 = (bf16[8,128]{1,0:T(8,128)(2,1)S(1)}, bf16[8,128]{1,0:T(8,128)(2,1)S(1)}, u32[]{:S(2)}, u32[]{:S(2)}) collective-permute-start(bf16[8,128]{1,0:T(8,128)(2,1)S(1)} %get-tuple-element.374), channel_id=1, source_target_pairs={{4,0},{8,4},{12,8},{16,12},{20,16},{24,20},{28,24},{32,28},{36,32}... | collective-permute-start | bytes 6152 | tf_op jit(solution)/shard_map/ppermute | solution.py:22
  288.9 38.4 %collective-permute-start = (bf16[8,128]{1,0:T(8,128)(2,1)S(1)}, bf16[8,128]{1,0:T(8,128)(2,1)S(1)}, u32[]{:S(2)}, u32[]{:S(2)}) collective-permute-start(bf16[8,128]{1,0:T(8,128)(2,1)S(1)} %get-tuple-element.373), channel_id=1, source_target_pairs={{0,4},{4,8},{8,12},{12,16},{16,20},{20,24},{24,28},{28,32},{32,36}... | collective-permute-start | bytes 6152 | tf_op jit(solution)/shard_map/ppermute | solution.py:19
  315.1 1.9 copy-start.16
  315.1 0.5 copy-start.18
  318.4 8.9 %slice-start = ((bf16[1024,1152]{1,0:T(8,128)(2,1)}), bf16[1024,128]{1,0:T(8,128)(2,1)S(1)}, s32[]{:S(2)}) async-start(bf16[1024,1152]{1,0:T(8,128)(2,1)} %copy-done.7), calls=%async_computation.3 | async-start | bytes 524288 | tf_op jit(solution)/shard_map/slice | solution.py:193
  318.4 8.9 %copy-start.22 = (f32[128]{0:T(128)S(1)}, f32[128]{0:T(128)}, u32[]{:S(2)}) copy-start(f32[128]{0:T(128)} %dynamic_slice.60) | copy-start | bytes 1540
  329.5 5.5 %copy-start.4 = (bf16[2,1024,128]{2,1,0:T(8,128)(2,1)S(1)}, bf16[2,1024,128]{2,1,0:T(8,128)(2,1)}, u32[]{:S(2)}) copy-start(bf16[2,1024,128]{2,1,0:T(8,128)(2,1)} %rev.22) | copy-start | bytes 1572868
  329.5 5.5 %copy-start.11 = (f32[2,1024,128]{1,2,0:T(8,128)S(1)}, f32[2,1024,128]{1,2,0:T(8,128)}, u32[]{:S(2)}) copy-start(f32[2,1024,128]{1,2,0:T(8,128)} %reshape.649) | copy-start | bytes 3145732
  329.5 5.5 %copy-start.19 = (f32[2]{0:T(128)S(1)}, f32[2]{0:T(128)}, u32[]{:S(2)}) copy-start(f32[2]{0:T(128)} %copy-done.18) | copy-start | bytes 28
  329.5 5.5 %copy-start.20 = (f32[2,2,128,128]{3,2,1,0:T(8,128)S(1)}, f32[2,2,128,128]{3,2,1,0:T(8,128)}, u32[]{:S(2)}) copy-start(f32[2,2,128,128]{3,2,1,0:T(8,128)} %param.36) | copy-start | bytes 786436
  335.0 13.6 %copy-start.2 = (bf16[128,2,8,128]{3,2,1,0:T(8,128)(2,1)S(1)}, bf16[128,2,8,128]{3,2,1,0:T(8,128)(2,1)}, u32[]{:S(2)}) copy-start(bf16[128,2,8,128]{3,2,1,0:T(8,128)(2,1)} %copy-done.1) | copy-start | bytes 1572868
  335.0 13.6 %copy-start.17 = (f32[2]{0:T(128)S(1)}, f32[2]{0:T(128)}, u32[]{:S(2)}) copy-start(f32[2]{0:T(128)} %copy-done.16) | copy-start | bytes 28
Sparse Core Ops, SparseCore 0:
  9.0 51.1 all-gather.8
  231.8 47.1 all-gather.10
where the time goes:
time: 390 us; the launch traced here: 384 us
  matrix products  134 us (34%)
  blocking collectives  86.9 us (22%)
  local copies, waits for them, and re-layouts  71.2 us (18%)
  waiting for transfers between devices  44.1 us (11%)
  other arithmetic  26.8 us (7%)
  between operations  14 us (4%)
  starting transfers between devices  5.59 us (1%)
    all_gather x3, blocking collectives, per_device(): gathered = lax.all_gather(stacked, 'sp', axis=0, tiled=True)  71.4 us
    all_gather x1, waiting for transfers between devices, per_device(): whole_rows = lax.all_gather(tokens, 'tp', axis=1, tiled=True)  43.3 us
    dot_general x16, matrix products, block_step(): jnp.einsum('hts,hsv->htv', scores, v_blk)  21.4 us
    dot_general x16, matrix products, block_step(): jnp.einsum('hsv,hsk->hvk', v_blk * weights[:, :, None], k_blk)  18.7 us
    dot_general x16, matrix products, block_step(): jnp.einsum('htd,hsd->hts', q_blk, k_blk)  16.9 us
    dot_general x16, matrix products, block_step(): jnp.einsum('hvk,htk->htv', memory, q_blk)  16.6 us
    dot_general x16, matrix products, block_step(): jnp.einsum('hk,htk->ht', normer, q_blk)  15.5 us
    all_to_all x1, blocking collectives, per_device(): owned = lax.all_to_all(mixed, 'tp', split_axis=0, concat_axis=1, tiled=True)  15.5 us
  transfers between devices with their start and end apart: 4, of which 1 were waited for; matrix products, arithmetic and copies ran while one was open for 8% of the time, Pallas kernels for 0%

commit v1 on v0

--- a/solution.py
+++ b/solution.py
@@ -181,7 +181,9 @@
     gate_in = lax.dynamic_slice_in_dim(input_gate_matrix, group_index * head_local, head_local, 2)
     gate_fg = lax.dynamic_slice_in_dim(forget_gate_matrix, group_index * head_local, head_local, 2)
     gate_weight = jnp.concatenate([gate_in, gate_fg], axis=1).reshape(model_width, 4 * head_local)
-    whole_rows = lax.all_gather(tokens, "tp", axis=1, tiled=True)
+    whole_rows = jnp.concatenate(
+        lax.all_to_all(jnp.stack([tokens] * lax.axis_size("tp")), "tp", 0, 0), axis=1
+    )
     floats = whole_rows.astype(jnp.float32)
     mean_row = jnp.sum(floats, axis=1) / model_width
     variance = jnp.sum(floats * floats, axis=1) / model_width - mean_row * mean_row

time: 390 us -> 408 us (1.046)
  local copies, waits for them, and re-layouts: 71.2 us -> 82.5 us
  waiting for transfers between devices: 44.1 us -> 39.7 us
  blocking collectives: 86.9 us -> 91.3 us
  starting transfers between devices: 5.59 us -> 9.92 us
  other arithmetic: 26.8 us -> 31.1 us
    all_gather x1 -> x0, waiting for transfers between devices: 43.3 us -> none  [per_device(): whole_rows = lax.all_gather(tokens, 'tp', axis=1, tiled=True)]
    all_to_all x0 -> x1, waiting for transfers between devices: none -> 39.7 us  [per_device(): lax.all_to_all(jnp.stack([tokens] * lax.axis_size('tp')), 'tp', 0, 0)]
    all_to_all x0 -> x1, local copies, waits for them, and re-layouts: none -> 6.31 us  [per_device(): lax.all_to_all(jnp.stack([tokens] * lax.axis_size('tp')), 'tp', 0, 0)]
    all_to_all x0 -> x1, starting transfers between devices: none -> 5.02 us  [per_device(): lax.all_to_all(jnp.stack([tokens] * lax.axis_size('tp')), 'tp', 0, 0)]
    all_gather x3, blocking collectives: 71.4 us -> 75.7 us  [per_device(): gathered = lax.all_gather(stacked, 'sp', axis=0, tiled=True)]
  transfers between devices with their start and end apart: 4 -> 4, of which waited for: 1 -> 1; matrix products, arithmetic and copies ran while one was open for 8% -> 7% of each run, Pallas kernels for 0% -> 0%
where the time goes in v1:
time: 408 us; the launch traced here: 400 us
  matrix products  132 us (32%)
  blocking collectives  91.3 us (22%)
  local copies, waits for them, and re-layouts  82.5 us (20%)
  waiting for transfers between devices  39.7 us (10%)
  other arithmetic  31.1 us (8%)
  between operations  14 us (3%)
  starting transfers between devices  9.92 us (2%)
    all_gather x3, blocking collectives, per_device(): gathered = lax.all_gather(stacked, 'sp', axis=0, tiled=True)  75.7 us
    all_to_all x1, waiting for transfers between devices, per_device(): lax.all_to_all(jnp.stack([tokens] * lax.axis_size('tp')), 'tp', 0, 0)  39.7 us
    dot_general x16, matrix products, block_step(): jnp.einsum('hts,hsv->htv', scores, v_blk)  21.4 us
    dot_general x16, matrix products, block_step(): jnp.einsum('hsv,hsk->hvk', v_blk * weights[:, :, None], k_blk)  18.7 us
    dot_general x16, matrix products, block_step(): jnp.einsum('htd,hsd->hts', q_blk, k_blk)  17.1 us
    dot_general x16, matrix products, block_step(): jnp.einsum('hvk,htk->htv', memory, q_blk)  16.2 us
    dot_general x16, matrix products, block_step(): jnp.einsum('hs,hsk->hk', weights, k_blk)  15.6 us
    all_to_all x1, blocking collectives, per_device(): owned = lax.all_to_all(mixed, 'tp', split_axis=0, concat_axis=1, tiled=True)  15.5 us
  transfers between devices with their start and end apart: 4, of which 1 were waited for; matrix products, arithmetic and copies ran while one was open for 7% of the time, Pallas kernels for 0%

profile of v1, /device:TPU:1, one launch (start us, length us, event | category | flops | bytes accessed | tf_op | source)
XLA Modules:
  0.0 400.5 jit_solution(15390025948402802978)
XLA Ops:
  6.5 3.7 stack.37
  10.2 5.0 %all-to-all-start = ((bf16[4,1024,512]{2,1,0:T(8,128)(2,1)}), bf16[4,1024,512]{2,1,0:T(8,128)(2,1)}, u32[]{:S(2)}, u32[]{:S(2)}) async-start(bf16[4,1024,512]{2,1,0:T(8,128)(2,1)} %stack.37), calls=%async_computation | async-start | bytes 8388608 | tf_op jit(solution)/shard_map/all_to_all | solution.py:185
  16.5 2.0 constant_dynamic-update-slice_fusion.8
  19.7 2.3 constant_dynamic-update-slice_fusion.6
  24.2 39.7 %all-to-all-done = bf16[4,1024,512]{2,1,0:T(8,128)(2,1)} async-done(((bf16[4,1024,512]{2,1,0:T(8,128)(2,1)}), bf16[4,1024,512]{2,1,0:T(8,128)(2,1)}, u32[]{:S(2)}, u32[]{:S(2)}) %all-to-all-start) | async-done | bytes 4194336 | tf_op jit(solution)/shard_map/all_to_all | solution.py:185
  63.9 6.3 %copy.123 = bf16[4,1024,512]{1,2,0:T(8,128)(2,1)} copy(bf16[4,1024,512]{2,1,0:T(8,128)(2,1)} %all-to-all-done) | data formatting | bytes 8388608 | tf_op jit(solution)/shard_map/all_to_all | solution.py:185
  70.2 3.5 convert_reduce_fusion
  73.8 2.7 fusion.68
  80.2 8.9 %convolution_convert_fusion = bf16[1024,1152]{1,0:T(8,128)(2,1)S(1)} fusion(bf16[1024,2048]{0,1:T(8,128)(2,1)} %fusion.68, bf16[2048,1152]{1,0:T(8,128)(2,1)} %constant_dynamic-update-slice_fusion.4), kind=kOutput, calls=%fused_computation.123 | convolution fusion | flops 4833017856 | bytes 11272192 | tf_op jit(solution)/shard_map/dot_general | solution.py:193
  90.9 5.1 %rev.20 = f32[2,1024,128]{2,1,0:T(8,128)} reverse(f32[2,1024,128]{2,1,0:T(8,128)S(1)} %bitcast.510), dimensions={1} | reverse | bytes 2097152 | tf_op jit(solution)/shard_map/rev | solution.py:227
  95.9 2.5 copy_bitcast_fusion
  98.5 8.2 %rev.22 = bf16[2,1024,128]{2,1,0:T(8,128)(2,1)} reverse(bf16[2,1024,128]{2,1,0:T(8,128)(2,1)} %get-tuple-element.431), dimensions={1} | reverse | bytes 1048576 | tf_op jit(solution)/shard_map/rev | solution.py:223
  106.7 1.9 copy.250
  108.6 8.2 %rev.21 = bf16[2,1024,128]{2,1,0:T(8,128)(2,1)} reverse(bf16[2,1024,128]{2,1,0:T(8,128)(2,1)} %get-tuple-element.405), dimensions={1} | reverse | bytes 1048576 | tf_op jit(solution)/shard_map/rev | solution.py:226
  117.9 65.9 %while.43 = (s32[]{:T(128)}, f32[2,128,128]{2,1,0:T(8,128)S(1)}, f32[2,128]{1,0:T(2,128)S(1)}, f32[2]{0:T(128)S(1)}, f32[8,2,128,128]{3,2,1,0:T(8,128)}, /*index...) while((s32[]{:T(128)}, f32[2,128,128]{2,1,0:T(8,128)S(1)}, ...), condition=%wide.region_18.19_spmd.clone, body=%wide.region_13.18_spmd.clone.sunk | while | flops 34327816 | bytes 1600317 | solution.py:75
  183.9 1.9 copy.251
  186.9 58.1 %while.42 = (s32[]{:T(128)}, f32[2,128,128]{2,1,0:T(8,128)S(1)}, f32[2,128]{1,0:T(2,128)S(1)}, f32[2]{0:T(128)S(1)}, f32[8,2,128,128]{3,2,1,0:T(8,128)}, /*index...) while((s32[]{:T(128)}, f32[2,128,128]{2,1,0:T(8,128)S(1)}, ...), condition=%wide.region_7.8_spmd.clone, body=%wide.region_2.7_spmd.clone.sunk | while | flops 34327816 | bytes 1600821 | solution.py:75
  249.6 27.5 %all-gather.4 = f32[32,2,2]{2,1,0:T(2,128)S(1)} all-gather(f32[1,2,2]{2,1,0:T(2,128)S(1)} %maximum_bitcast_fusion), channel_id=2, replica_groups=mesh['sp'=32,'tp'=4] {'sp'}, dimensions={0}, use_global_device_ids=true | all-gather | bytes 528 | tf_op jit(solution)/shard_map/all_gather | solution.py:257
  278.2 2.9 collective-permute-start
  281.2 1.9 collective-permute-start.1
  283.2 26.7 %all-gather.5 = f32[32,2,2]{2,1,0:T(2,128)S(1)} all-gather(f32[1,2,2]{2,1,0:T(2,128)S(1)} %maximum_bitcast_fusion.1), channel_id=3, replica_groups=mesh['sp'=32,'tp'=4] {'sp'}, dimensions={0}, use_global_device_ids=true | all-gather | bytes 528 | tf_op jit(solution)/shard_map/all_gather | solution.py:257
  310.5 21.5 %all-gather.3 = bf16[64,2,128]{2,1,0:T(2,128)(2,1)S(1)} all-gather(bf16[2,2,128]{2,1,0:T(2,128)(2,1)S(1)} %pad_maximum_fusion.3), channel_id=5, replica_groups=mesh['sp'=32,'tp'=4] {'sp'}, dimensions={0}, use_global_device_ids=true | all-gather | bytes 33792 | tf_op jit(solution)/shard_map/all_gather | solution.py:257
  335.4 2.6 copy.146
  338.0 2.4 reshape.667
  341.8 2.4 reshape.670
  344.2 2.1 fusion.79
  346.3 4.2 %slice_bitcast_fusion.1 = (bf16[32,2,128,128]{3,2,1,0:T(8,128)(2,1)}, bf16[32,2,128,128]{3,2,1,0:T(8,128)(2,1)S(1)}) fusion(bf16[32,2,2,128,128]{4,3,2,1,0:T(8,128)(2,1)} %bitcast.514), kind=kLoop, calls=%fused_computation.118 | loop fusion | bytes 8388608 | tf_op jit(solution)/shard_map/squeeze | solution.py:258
  353.2 9.4 %rev.23 = f32[2,1024,128]{1,2,0:T(8,128)} reverse(f32[2,1024,128]{1,2,0:T(8,128)} %fusion.78), dimensions={1} | reverse | bytes 2097152 | tf_op jit(solution)/shard_map/rev | solution.py:271
  362.6 2.8 fusion.71
  365.4 2.0 fusion.171
  372.9 15.5 %all_to_all.21 = bf16[4,256,384]{1,2,0:T(8,128)(2,1)S(1)} all-to-all(bf16[4,256,384]{1,2,0:T(8,128)(2,1)} %copy.155), channel_id=1, replica_groups=mesh['sp'=32,'tp'=4] {'tp'}, dimensions={0} | all-to-all | bytes 1572864 | tf_op jit(solution)/shard_map/all_to_all | solution.py:283
  388.5 3.5 fusion.174
  (430 shorter events, 156.5 us)
Async XLA Ops:
  6.5 385.4 %copy-start = (bf16[512,2048]{1,0:T(8,128)(2,1)S(1)}, bf16[512,2048]{1,0:T(8,128)(2,1)}, u32[]{:S(2)}) copy-start(bf16[512,2048]{1,0:T(8,128)(2,1)} %param.42) | copy-start | bytes 6291460
  10.2 5.1 %copy-start.10 = (f32[2048]{0:T(1024)S(1)}, f32[2048]{0:T(1024)}, u32[]{:S(2)}) copy-start(f32[2048]{0:T(1024)} %param.25) | copy-start | bytes 24580
  10.2 6.2 %copy-start.14 = (f32[2,8]{1,0:T(2,128)S(1)}, f32[2,8]{1,0:T(2,128)}, u32[]{:S(2)}) copy-start(f32[2,8]{1,0:T(2,128)} %param.33) | copy-start | bytes 196
  10.2 8.3 %copy-start.6 = (bf16[2048,256]{1,0:T(8,128)(2,1)S(1)}, bf16[2048,256]{1,0:T(8,128)(2,1)}, u32[]{:S(2)}) copy-start(bf16[2048,256]{1,0:T(8,128)(2,1)} %param.27) | copy-start | bytes 3145732
  10.2 53.7 %all-to-all-start = ((bf16[4,1024,512]{2,1,0:T(8,128)(2,1)}), bf16[4,1024,512]{2,1,0:T(8,128)(2,1)}, u32[]{:S(2)}, u32[]{:S(2)}) async-start(bf16[4,1024,512]{2,1,0:T(8,128)(2,1)} %stack.37), calls=%async_computation | async-start | bytes 8388608 | tf_op jit(solution)/shard_map/all_to_all | solution.py:185
  15.3 331.0 %all-gather.8.cloned.1.call-start = ((), (), s32[]{:S(2)}) async-start(), calls=%async_computation.2 | async-start | bytes 4325376 | tf_op jit(solution)/shard_map/all_gather | solution.py:257
  16.4 5.5 %copy-start.7 = (bf16[2048,256]{1,0:T(8,128)(2,1)S(1)}, bf16[2048,256]{1,0:T(8,128)(2,1)}, u32[]{:S(2)}) copy-start(bf16[2048,256]{1,0:T(8,128)(2,1)} %param.29) | copy-start | bytes 3145732
  16.5 6.6 %copy-start.8 = (bf16[2048,256]{1,0:T(8,128)(2,1)S(1)}, bf16[2048,256]{1,0:T(8,128)(2,1)}, u32[]{:S(2)}) copy-start(bf16[2048,256]{1,0:T(8,128)(2,1)} %param.30) | copy-start | bytes 3145732
  70.2 3.5 copy-start.1
  77.8 1.6 copy-start.11
  77.8 1.6 copy-start.12
  89.1 1.8 copy-start.5
  186.9 123.3 %copy-start.15 = (f32[2,2]{1,0:T(2,128)S(1)}, f32[2,2]{1,0:T(2,128)}, u32[]{:S(2)}) copy-start(f32[2,2]{1,0:T(2,128)} %param.38) | copy-start | bytes 52
  186.9 145.5 %copy-start.13 = (f32[2,2,128]{2,1,0:T(2,128)S(1)}, f32[2,2,128]{2,1,0:T(2,128)}, u32[]{:S(2)}) copy-start(f32[2,2,128]{2,1,0:T(2,128)} %param.37) | copy-start | bytes 6148
  244.9 95.6 %copy-start.4 = (f32[8,2,128,128]{3,2,1,0:T(8,128)S(1)}, f32[8,2,128,128]{3,2,1,0:T(8,128)}, u32[]{:S(2)}) copy-start(f32[8,2,128,128]{3,2,1,0:T(8,128)} %get-tuple-element.149) | copy-start | bytes 3145732
  278.2 65.9 %collective-permute-start = (bf16[8,128]{1,0:T(8,128)(2,1)S(1)}, bf16[8,128]{1,0:T(8,128)(2,1)S(1)}, u32[]{:S(2)}, u32[]{:S(2)}) collective-permute-start(bf16[8,128]{1,0:T(8,128)(2,1)S(1)} %get-tuple-element.397), channel_id=1, source_target_pairs={{0,4},{4,8},{8,12},{12,16},{16,20},{20,24},{24,28},{28,32},{32,36}... | collective-permute-start | bytes 6152 | tf_op jit(solution)/shard_map/ppermute | solution.py:19
  281.2 63.0 %collective-permute-start.1 = (bf16[8,128]{1,0:T(8,128)(2,1)S(1)}, bf16[8,128]{1,0:T(8,128)(2,1)S(1)}, u32[]{:S(2)}, u32[]{:S(2)}) collective-permute-start(bf16[8,128]{1,0:T(8,128)(2,1)S(1)} %get-tuple-element.398), channel_id=1, source_target_pairs={{4,0},{8,4},{12,8},{16,12},{20,16},{24,20},{28,24},{32,28},{36,32}... | collective-permute-start | bytes 6152 | tf_op jit(solution)/shard_map/ppermute | solution.py:22
  335.4 8.7 %slice-start = ((bf16[1024,1152]{1,0:T(8,128)(2,1)}), bf16[1024,128]{1,0:T(8,128)(2,1)S(1)}, s32[]{:S(2)}) async-start(bf16[1024,1152]{1,0:T(8,128)(2,1)} %copy-done.5), calls=%async_computation.3 | async-start | bytes 524288 | tf_op jit(solution)/shard_map/slice | solution.py:195
  346.3 5.5 %copy-start.3 = (bf16[2,1024,128]{2,1,0:T(8,128)(2,1)S(1)}, bf16[2,1024,128]{2,1,0:T(8,128)(2,1)}, u32[]{:S(2)}) copy-start(bf16[2,1024,128]{2,1,0:T(8,128)(2,1)} %rev.22) | copy-start | bytes 1572868
  346.3 5.5 %copy-start.9 = (f32[2,1024,128]{1,2,0:T(8,128)S(1)}, f32[2,1024,128]{1,2,0:T(8,128)}, u32[]{:S(2)}) copy-start(f32[2,1024,128]{1,2,0:T(8,128)} %reshape.670) | copy-start | bytes 3145732
  346.3 5.5 %copy-start.16 = (f32[2,2,128,128]{3,2,1,0:T(8,128)S(1)}, f32[2,2,128,128]{3,2,1,0:T(8,128)}, u32[]{:S(2)}) copy-start(f32[2,2,128,128]{3,2,1,0:T(8,128)} %param.36) | copy-start | bytes 786436
  351.8 13.6 %copy-start.2 = (bf16[128,2,8,128]{3,2,1,0:T(8,128)(2,1)S(1)}, bf16[128,2,8,128]{3,2,1,0:T(8,128)(2,1)}, u32[]{:S(2)}) copy-start(bf16[128,2,8,128]{3,2,1,0:T(8,128)(2,1)} %get-tuple-element.400) | copy-start | bytes 1572868
Sparse Core Ops, SparseCore 0:
  245.7 48.4 all-gather.7
